TPU v7x, 32 devices: a whole 2x2x4 slice. The times are simulated.
32 devices in a mesh: rep: 4 (over z), fs: 4 (over y, x), tp: 2 (over core).
Axes of the slice: x: 2, y: 2, z: 4, core: 2. Of those that a mesh axis runs over, the one named last changes fastest.
Arguments:
- tokens: bfloat16 [2048, 1024], P(('rep', 'fs', 'tp')), may hold values from -6 to 6
- cotangent: bfloat16 [2048, 1024], P(('rep', 'fs', 'tp')), may hold values from -6 to 6
- gate_weight: bfloat16 [1024, 2816], P('fs', 'tp'), may hold values from -0.1875 to 0.1875
- up_weight: bfloat16 [1024, 2816], P('fs', 'tp'), may hold values from -0.1875 to 0.1875
- down_weight: bfloat16 [2816, 1024], P('tp', 'fs'), may hold values from -0.109375 to 0.109375
Outputs:
- input_grad: bfloat16 [2048, 1024], P(('rep', 'fs', 'tp'))
- gate_grad: float32 [1024, 2816], P('fs', 'tp')
- up_grad: float32 [1024, 2816], P('fs', 'tp')
- down_grad: float32 [2816, 1024], P('tp', 'fs')
- gate_power: float32 [1024], P('fs')
- up_power: float32 [1024], P('fs')
- down_power: float32 [2816], P('tp')
All inputs are finite; a program needn't handle non-finite values.
Results may differ from a plain program's by a relative error of at most 0.0017.
Values may be sent and summed in bfloat16 or wider, within the bound.
A program may use at most 64 MiB of HBM per device.

v0:
```python
import math

import jax
import jax.numpy as jnp
from jax import lax
from jax.sharding import PartitionSpec as P

D = 1024
FF = 2816


EPSILON = 1e-06


def contract_rows(left, right):
    return lax.dot_general(
        left, right, (((0,), (0,)), ((), ())), preferred_element_type=jnp.float32
    )


def contract_cols(left, right):
    return lax.dot_general(
        left, right, (((1,), (1,)), ((), ())), preferred_element_type=jnp.float32
    )


def on_device(tokens, cotangent, gate_weight, up_weight, down_weight):
    tp_count = lax.axis_size("tp")
    fs_count = lax.axis_size("fs")
    rep_count = lax.axis_size("rep")
    width = tokens.shape[1]
    factor = 1.0 / math.sqrt(tokens.shape[0] * tp_count * fs_count * rep_count)
    xfloat = tokens.astype(jnp.float32)
    recip_norm = lax.rsqrt(jnp.mean(xfloat * xfloat, axis=1, keepdims=True) + EPSILON)
    normed_exact = xfloat * recip_norm
    normed = normed_exact.astype(jnp.bfloat16)
    group_normed, group_cotangent = (
        lax.all_gather(normed, "tp", axis=0, tiled=True),
        lax.all_gather(cotangent, "tp", axis=0, tiled=True),
    )
    gate_full, up_full, down_full = (
        lax.all_gather(gate_weight, "fs", axis=0, tiled=True),
        lax.all_gather(up_weight, "fs", axis=0, tiled=True),
        lax.all_gather(down_weight.T, "fs", axis=0, tiled=True),
    )
    gate_pre = jnp.dot(group_normed, gate_full, preferred_element_type=jnp.float32)
    up_pre = jnp.dot(group_normed, up_full, preferred_element_type=jnp.float32)
    sigmoid_gate = jax.nn.sigmoid(gate_pre)
    activated = gate_pre * sigmoid_gate
    hidden = (activated * up_pre).astype(jnp.bfloat16)
    grad_hidden = 0.5 * jnp.dot(group_cotangent, down_full, preferred_element_type=jnp.float32)
    grad_up_pre = (grad_hidden * activated).astype(jnp.bfloat16)
    grad_gate_pre = (
        grad_hidden * up_pre * sigmoid_gate * (1.0 + gate_pre * (1.0 - sigmoid_gate))
    ).astype(jnp.bfloat16)
    normed_part = contract_cols(grad_gate_pre, gate_full) + contract_cols(grad_up_pre, up_full)
    grad_normed = lax.psum_scatter(normed_part, "tp", scatter_dimension=0, tiled=True)
    inner = jnp.mean(grad_normed * normed_exact, axis=1, keepdims=True)
    input_grad = (recip_norm * (grad_normed - normed_exact * inner)).astype(jnp.bfloat16)
    hidden_local = gate_weight.shape[1]

    def rows_term():
        normed_cols = lax.slice_in_dim(
            group_normed, 0, width // fs_count * lax.axis_size("fs"), axis=1
        )
        cotangent_cols = lax.slice_in_dim(
            group_cotangent, 0, width // fs_count * lax.axis_size("fs"), axis=1
        )
        return factor * jnp.concatenate(
            [
                contract_rows(normed_cols, grad_gate_pre),
                contract_rows(normed_cols, grad_up_pre),
                0.5 * contract_rows(cotangent_cols, hidden),
            ],
            axis=1,
        )

    reduced = lax.psum_scatter(rows_term(), "fs", scatter_dimension=0, tiled=True)
    reduced = lax.psum(reduced, "rep")
    gate_grad = reduced[:, :hidden_local]
    up_grad = reduced[:, hidden_local : 2 * hidden_local]
    down_grad = reduced[:, 2 * hidden_local :].T
    gate_sums, up_sums = lax.psum(
        (jnp.sum(gate_grad * gate_grad, axis=1), jnp.sum(up_grad * up_grad, axis=1)), "tp"
    )
    down_sums = lax.psum(jnp.sum(down_grad * down_grad, axis=1), "fs")
    return (input_grad, gate_grad, up_grad, down_grad, gate_sums / FF, up_sums / FF, down_sums / D)


def solution(mesh):
    placed = (
        P(("rep", "fs", "tp"), None),
        P(("rep", "fs", "tp"), None),
        P("fs", "tp"),
        P("fs", "tp"),
        P("tp", "fs"),
    )
    return jax.shard_map(
        on_device,
        mesh=mesh,
        in_specs=placed,
        out_specs=(
            P(("rep", "fs", "tp"), None),
            P("fs", "tp"),
            P("fs", "tp"),
            P("tp", "fs"),
            P("fs"),
            P("fs"),
            P("tp"),
        ),
        check_vma=False,
    )
```

profile of v0, /device:TPU:0, one launch (start us, length us, event | category | flops | bytes accessed | tf_op | source)
XLA Modules:
  0.0 511.1 jit_solution(5771994517067918810)
XLA Ops:
  7.2 0.7 all-gather.8.cloned.1.call-update
  8.0 0.7 all-gather.6.cloned.1.call-update
  8.7 0.7 all-gather.4.cloned.1.call-update
  9.4 1.0 fusion.8
  10.5 1.0 fusion.3
  11.5 2.1 all_gather.17
  13.6 2.0 all_gather.15
  15.6 38.5 %all-gather.8.cloned.1.call-done = bf16[1024,1408]{1,0:T(8,128)(2,1)} async-done(((bf16[256,1408]{1,0:T(8,128)(2,1)}), bf16[1024,1408]{1,0:T(8,128)(2,1)}) %all-gather.8.cloned.1.call-update) | async-done | bytes 2883600 | tf_op jit(solution)/shard_map/all_gather | solution.py:42
  54.1 2.4 fusion.12
  56.5 40.9 %all-gather.6.cloned.1.call-done = bf16[1024,1408]{1,0:T(8,128)(2,1)} async-done(((bf16[256,1408]{1,0:T(8,128)(2,1)}), bf16[1024,1408]{1,0:T(8,128)(2,1)}) %all-gather.6.cloned.1.call-update) | async-done | bytes 2883600 | tf_op jit(solution)/shard_map/all_gather | solution.py:43
  97.4 2.4 fusion.11
  99.8 3.5 multiply_bitcast_fusion
  103.3 37.3 %all-gather.4.cloned.1.call-done = bf16[1024,1408]{0,1:T(8,128)(2,1)} async-done(((bf16[256,1408]{0,1:T(8,128)(2,1)}), bf16[1024,1408]{0,1:T(8,128)(2,1)}) %all-gather.4.cloned.1.call-update) | async-done | bytes 2883600 | tf_op jit(solution)/shard_map/all_gather | solution.py:44
  140.6 2.9 multiply_convert_fusion.1
  143.6 0.9 fusion.15
  144.5 0.9 fusion.14
  145.5 1.2 slice-done
  147.2 6.3 %maximum_multiply_fusion = f32[1024,4224]{1,0:T(8,128)} fusion(f32[1024,1408]{1,0:T(8,128)S(1)} %bitcast.23, f32[1024,1408]{1,0:T(8,128)S(1)} %fusion.15, f32[1024,1408]{1,0:T(8,128)S(1)} %fusion.14), kind=kLoop, calls=%fused_computation | loop fusion | flops 12976128 | bytes 34603008 | tf_op jit(solution)/shard_map/mul | solution.py:69
  153.6 1.7 copy-done
  155.3 1.0 fusion.13
  156.4 0.8 copy-done.1
  157.1 1.8 convolution_add_fusion
  159.1 152.4 %reduce-scatter.5.cloned.1.call-done = f32[256,4224]{1,0:T(8,128)} async-done(((f32[1024,4224]{1,0:T(8,128)}), f32[256,4224]{1,0:T(8,128)}) %reduce-scatter.5.cloned.1.call-update) | async-done | bytes 4325392 | tf_op jit(solution)/shard_map/reduce_scatter | solution.py:78
  311.5 10.6 %reduce-scatter.3.cloned.1.call-done = f32[64,1024]{1,0:T(8,128)} async-done(((f32[128,1024]{1,0:T(8,128)}), f32[64,1024]{1,0:T(8,128)}) %reduce-scatter.3.cloned.1.call-update) | async-done | bytes 262160 | tf_op jit(solution)/shard_map/reduce_scatter | solution.py:57
  322.1 1.2 fusion.4
  323.2 1.7 fusion.7
  325.0 158.7 %all-reduce.3.cloned.1.call-done = f32[256,4224]{1,0:T(8,128)} async-done(((f32[256,4224]{1,0:T(8,128)}), f32[256,4224]{1,0:T(8,128)}) %all-reduce.3.cloned.1.call-update) | async-done | bytes 4325392 | tf_op jit(solution)/shard_map/psum | solution.py:79
  483.7 1.5 multiply_reduce_fusion
  485.1 10.0 %psum.31 = f32[1408]{0:T(1024)S(1)} all-reduce(f32[1408]{0:T(1024)S(1)} %multiply_reduce_fusion), channel_id=1, replica_groups=mesh['rep'=4,'fs'=4,'tp'=2] {'fs'}, use_global_device_ids=true, to_apply=%region_10.0 | all-reduce | flops 1408 | bytes 11264 | tf_op jit(solution)/shard_map/psum | solution.py:86
  495.7 3.9 multiply_reduce_fusion.1
  499.7 1.5 copy.13
  501.2 2.4 all-reduce
  (27 shorter events, 2.0 us)
Async XLA Ops:
  7.2 6.5 %copy-start.5 = (bf16[64,1024]{1,0:T(8,128)(2,1)S(1)}, bf16[64,1024]{1,0:T(8,128)(2,1)}, u32[]{:S(2)}) copy-start(bf16[64,1024]{1,0:T(8,128)(2,1)} %param.6) | copy-start | bytes 393220
  7.2 46.9 %all-gather.8.cloned.1.call-start = ((), (), s32[]{:S(2)}) async-start(), calls=%async_computation.4 | async-start | bytes 3604480 | tf_op jit(solution)/shard_map/all_gather | solution.py:42
  7.9 89.5 %all-gather.6.cloned.1.call-start = ((), (), s32[]{:S(2)}) async-start(), calls=%async_computation.3 | async-start | bytes 3604480 | tf_op jit(solution)/shard_map/all_gather | solution.py:43
  8.7 131.9 %all-gather.4.cloned.1.call-start = ((), (), s32[]{:S(2)}) async-start(), calls=%async_computation.2 | async-start | bytes 3604480 | tf_op jit(solution)/shard_map/all_gather | solution.py:44
  9.4 302.0 %reduce-scatter.5.cloned.1.call-start = ((), (), s32[]{:S(2)}) async-start(), calls=%async_computation.6 | async-start | bytes 21626880 | tf_op jit(solution)/shard_map/reduce_scatter | solution.py:78
  143.5 1.0 copy-start.3
  144.5 2.2 slice-start
  144.5 2.7 slice-start.1
  153.5 1.8 copy-start
  153.5 168.6 %reduce-scatter.3.cloned.1.call-start = ((), (), s32[]{:S(2)}) async-start(), calls=%async_computation.5 | async-start | bytes 786432 | tf_op jit(solution)/shard_map/reduce_scatter | solution.py:57
  155.3 1.8 copy-start.1
  155.3 1.8 copy-start.4
  159.0 163.1 %copy-start.2 = (bf16[64,1024]{1,0:T(8,128)(2,1)S(1)}, bf16[64,1024]{1,0:T(8,128)(2,1)}, u32[]{:S(2)}) copy-start(bf16[64,1024]{1,0:T(8,128)(2,1)} %param.5) | copy-start | bytes 393220
  159.0 324.6 %all-reduce.3.cloned.1.call-start = ((), (), s32[]{:S(2)}) async-start(), calls=%async_computation.7 | async-start | bytes 8650752 | tf_op jit(solution)/shard_map/psum | solution.py:79
Sparse Core Ops, SparseCore 0:
  9.8 44.2 all-gather.7
  55.9 41.4 all-gather.5
  99.2 41.3 all-gather.3
  153.6 157.7 reduce-scatter.4
  314.1 7.9 reduce-scatter.2
  324.3 159.3 all-reduce.2
where the time goes:
time: 512 us; the launch traced here: 511 us
  waiting for transfers between devices  440 us (86%)
  other arithmetic  17.8 us (3%)
  blocking collectives  16.6 us (3%)
  matrix products  16 us (3%)
  between operations  14.2 us (3%)
  local copies, waits for them, and re-layouts  5.81 us (1%)
    psum x1, waiting for transfers between devices, on_device(): reduced = lax.psum(reduced, 'rep')  159 us
    reduce_scatter x1, waiting for transfers between devices, on_device(): lax.psum_scatter(rows_term(), 'fs', scatter_dimension=0, tiled=True)  152 us
    all_gather x1, waiting for transfers between devices, on_device(): lax.all_gather(up_weight, 'fs', axis=0, tiled=True)  40.9 us
    all_gather x1, waiting for transfers between devices, on_device(): lax.all_gather(gate_weight, 'fs', axis=0, tiled=True)  38.5 us
    all_gather x1, waiting for transfers between devices, on_device(): lax.all_gather(down_weight.T, 'fs', axis=0, tiled=True)  37.3 us
    reduce_scatter x1, waiting for transfers between devices, on_device(): lax.psum_scatter(normed_part, 'tp', scatter_dimension=0, tiled=True)  10.6 us
  transfers between devices with their start and end apart: 6, of which 6 were waited for; matrix products, arithmetic and copies ran while one was open for 3% of the time, Pallas kernels for 0%

commit v1 on v0

--- a/solution.py
+++ b/solution.py
@@ -1,8 +1,11 @@
+import functools
 import math
 
 import jax
 import jax.numpy as jnp
 from jax import lax
+from jax.experimental import pallas as pl
+from jax.experimental.pallas import tpu as pltpu
 from jax.sharding import PartitionSpec as P
 
 D = 1024
@@ -87,6 +90,431 @@
     return (input_grad, gate_grad, up_grad, down_grad, gate_sums / FF, up_sums / FF, down_sums / D)
 
 
+MESH = pl.DeviceIdType.MESH
+GATE, UP, DOWN = 0, 1, 2
+
+
+def exchange_kernel(
+    n_rep, n_fs, factor,
+    tokens_ref, cotangent_ref, gate_ref, up_ref, down_ref,
+    input_ref, gate_out, up_out, down_out, column_power, row_power,
+    rows_all, gate_all, up_all, down_all,
+    grad_gate, grad_up, hidden_all,
+    normed_part, partner_part, rep_part,
+    gate_send, up_send, down_send, gate_recv, up_recv, down_recv,
+    column_parts, row_parts,
+    rows_up, rows_down, rows_recv, pair_send, pair_recv,
+    weight_ssem, weight_rsem,
+    partner_ssem, partner_rsem, rep_ssem, rep_rsem,
+    scatter_ssem, scatter_rsem,
+    gather_up, gather_down, gather_rsem,
+    column_ssem, column_rsem, row_ssem, row_rsem,
+):
+    z, f, t = lax.axis_index("rep"), lax.axis_index("fs"), lax.axis_index("tp")
+    other = 1 - t
+    local, width = tokens_ref.shape
+    block = gate_ref.shape[0]
+    hidden_units = gate_ref.shape[1]
+    chunk = 2 * local
+
+    def remote(source, target, send_sem, recv_sem, where):
+        return pltpu.make_async_remote_copy(
+            src_ref=source, dst_ref=target, send_sem=send_sem, recv_sem=recv_sem,
+            device_id={"rep": where[0], "fs": where[1], "tp": where[2]},
+            device_id_type=MESH,
+        )
+
+    def shifted(value, by, count):
+        return lax.rem(value + by, count)
+
+    barrier = pltpu.get_barrier_semaphore()
+
+    def greet(where):
+        pl.semaphore_signal(
+            barrier, inc=1, device_id={"rep": where[0], "fs": where[1], "tp": where[2]},
+            device_id_type=MESH,
+        )
+
+    for dz in range(n_rep):
+        for df in range(n_fs):
+            if dz or df:
+                greet((shifted(z, dz, n_rep), shifted(f, df, n_fs), t))
+        greet((shifted(z, dz, n_rep), f, other))
+
+    def normalise():
+        xfloat = tokens_ref[...].astype(jnp.float32)
+        mean = jnp.sum(xfloat * xfloat, axis=1, keepdims=True) * (1.0 / width)
+        recip_norm = lax.rsqrt(mean + EPSILON)
+        return xfloat * recip_norm, recip_norm
+
+    rows_all[z, t, 0] = normalise()[0].astype(jnp.bfloat16)
+    rows_all[z, t, 1] = cotangent_ref[...]
+    gate_all[f] = gate_ref[...]
+    up_all[f] = up_ref[...]
+    down_all[f] = down_ref[...]
+    pl.semaphore_wait(barrier, n_rep * n_fs - 1 + n_rep)
+
+    weights = ((gate_ref, gate_all), (up_ref, up_all), (down_ref, down_all))
+
+    def weight_copy(which, d):
+        source, target = weights[which]
+        return remote(
+            source, target.at[f], weight_ssem.at[which, d], weight_rsem.at[which, d],
+            (z, shifted(f, d, n_fs), t),
+        )
+
+    def weight_arrival(which, d):
+        source, target = weights[which]
+        return remote(
+            source, target.at[shifted(f, n_fs - d, n_fs)],
+            weight_ssem.at[which, d], weight_rsem.at[which, d], (z, shifted(f, d, n_fs), t),
+        )
+
+    def row_copy(j, sems, to):
+        return remote(
+            rows_all.at[j, t], rows_all.at[j, t], sems.at[j], rows_recv.at[j], (to, f, t)
+        )
+
+    def pair_copy(j, half):
+        return remote(
+            rows_all.at[j, half], rows_all.at[j, half], pair_send.at[j], pair_recv.at[j],
+            (z, f, other),
+        )
+
+    @pl.when(z < n_rep - 1)
+    def _():
+        row_copy(z, rows_up, z + 1).start()
+
+    @pl.when(z > 0)
+    def _():
+        row_copy(z, rows_down, z - 1).start()
+
+    for which in (GATE, UP, DOWN):
+        for d in range(1, n_fs):
+            weight_copy(which, d).start()
+    pair_copy(z, t).start()
+
+    for s in range(1, n_rep):
+        @pl.when(z - s >= 0)
+        def _():
+            row_copy(z - s, rows_up, z).wait_recv()
+            pair_copy(z - s, t).start()
+
+            @pl.when(z < n_rep - 1)
+            def _():
+                row_copy(z - s, rows_up, z + 1).start()
+
+        @pl.when(z + s < n_rep)
+        def _():
+            row_copy(z + s, rows_down, z).wait_recv()
+            pair_copy(z + s, t).start()
+
+            @pl.when(z > 0)
+            def _():
+                row_copy(z + s, rows_down, z - 1).start()
+
+    for j in range(n_rep):
+        pair_copy(j, other).wait_recv()
+    for which in (GATE, UP, DOWN):
+        for d in range(1, n_fs):
+            weight_arrival(which, d).wait_recv()
+
+    def forward(j, carry):
+        normed = rows_all[j, :, 0].reshape(chunk, width)
+        cotangent = rows_all[j, :, 1].reshape(chunk, width)
+        gate_pre = jnp.dot(
+            normed, gate_all[...].reshape(width, hidden_units), preferred_element_type=jnp.float32
+        )
+        up_pre = jnp.dot(
+            normed, up_all[...].reshape(width, hidden_units), preferred_element_type=jnp.float32
+        )
+        grad_hidden = jnp.zeros((chunk, hidden_units), jnp.float32)
+        for k in range(n_fs):
+            grad_hidden += contract_cols(cotangent[:, k * block : (k + 1) * block], down_all[k])
+        grad_hidden = 0.5 * grad_hidden
+        sigmoid_gate = jax.nn.sigmoid(gate_pre)
+        activated = gate_pre * sigmoid_gate
+        at = pl.ds(pl.multiple_of(j * chunk, chunk), chunk)
+        hidden_all[at, :] = (activated * up_pre).astype(jnp.bfloat16)
+        grad_up_pre = (grad_hidden * activated).astype(jnp.bfloat16)
+        grad_gate_pre = (
+            grad_hidden * up_pre * sigmoid_gate * (1.0 + gate_pre * (1.0 - sigmoid_gate))
+        ).astype(jnp.bfloat16)
+        grad_up[at, :] = grad_up_pre
+        grad_gate[at, :] = grad_gate_pre
+        for k in range(n_fs):
+            part = contract_cols(grad_gate_pre, gate_all[k]) + contract_cols(
+                grad_up_pre, up_all[k]
+            )
+            normed_part[j, :, :, k * block : (k + 1) * block] = part.reshape(2, local, block)
+        return carry
+
+    lax.fori_loop(0, n_rep, forward, 0)
+
+    def partner_copy(j):
+        return remote(
+            normed_part.at[j, other], partner_part.at[j], partner_ssem.at[j], partner_rsem.at[j],
+            (z, f, other),
+        )
+
+    for j in range(n_rep):
+        partner_copy(j).start()
+
+    def columns_of(half, k):
+        at = pl.ds(pl.multiple_of(k * block, block), block)
+        return rows_all[:, :, half, :, at].reshape(n_rep * chunk, block)
+
+    def term(which, k):
+        if which == GATE:
+            return contract_rows(columns_of(0, k), grad_gate[...])
+        if which == UP:
+            return contract_rows(columns_of(0, k), grad_up[...])
+        return contract_rows(hidden_all[...], columns_of(1, k))
+
+    sums = ((gate_send, gate_recv), (up_send, up_recv), (down_send, down_recv))
+
+    def scatter_copy(which, d):
+        source, target = sums[which]
+        return remote(
+            source.at[d], target.at[d], scatter_ssem.at[which, d], scatter_rsem.at[which, d],
+            (z, shifted(f, d, n_fs), t),
+        )
+
+    def send_terms(which):
+        for d in range(1, n_fs):
+            sums[which][0][d] = term(which, shifted(f, d, n_fs))
+            scatter_copy(which, d).start()
+
+    def rep_copy(d):
+        return remote(
+            normed_part.at[shifted(z, d, n_rep), t], rep_part.at[d],
+            rep_ssem.at[d], rep_rsem.at[d], (shifted(z, d, n_rep), f, t),
+        )
+
+    send_terms(GATE)
+    for j in range(n_rep):
+        partner_copy(j).wait_recv()
+        normed_part[j, t] = normed_part[j, t] + partner_part[j]
+    for d in range(1, n_rep):
+        rep_copy(d).start()
+    send_terms(UP)
+    send_terms(DOWN)
+    for which in (GATE, UP, DOWN):
+        sums[which][0][0] = term(which, f)
+
+    outs = (gate_out, up_out, down_out)
+
+    def gather_copy(which, j, sems, to):
+        return remote(
+            outs[which].at[j], outs[which].at[j], sems.at[which, j], gather_rsem.at[which, j],
+            (to, f, t),
+        )
+
+    def row_squares(value):
+        return lax.dot_general(
+            jnp.ones((8, value.shape[1]), jnp.float32), value * value,
+            (((1,), (1,)), ((), ())), preferred_element_type=jnp.float32,
+            precision=lax.Precision.HIGHEST,
+        )
+
+    def own_sum(which):
+        source, target = sums[which]
+        total = source[0]
+        for d in range(1, n_fs):
+            scatter_copy(which, d).wait_recv()
+            total = total + target[d]
+        total = total * (factor if which != DOWN else 0.5 * factor)
+        outs[which][z] = total
+
+        @pl.when(z < n_rep - 1)
+        def _():
+            gather_copy(which, z, gather_up, z + 1).start()
+
+        @pl.when(z > 0)
+        def _():
+            gather_copy(which, z, gather_down, z - 1).start()
+
+        if which == DOWN:
+            row_parts[z, f] = row_squares(total)
+        else:
+            column_parts[z, t, which] = row_squares(total)
+
+    def relay(which, s):
+        @pl.when(z - s >= 0)
+        def _():
+            gather_copy(which, z - s, gather_up, z).wait_recv()
+
+            @pl.when(z < n_rep - 1)
+            def _():
+                gather_copy(which, z - s, gather_up, z + 1).start()
+
+        @pl.when(z + s < n_rep)
+        def _():
+            gather_copy(which, z + s, gather_down, z).wait_recv()
+
+            @pl.when(z > 0)
+            def _():
+                gather_copy(which, z + s, gather_down, z - 1).start()
+
+    def column_copy(dz, dt):
+        return remote(
+            column_parts.at[z, t], column_parts.at[z, t],
+            column_ssem.at[dz, dt], column_rsem.at[dz, dt],
+            (shifted(z, dz, n_rep), f, shifted(t, dt, 2)),
+        )
+
+    def column_arrival(dz, dt):
+        at_z, at_t = shifted(z, n_rep - dz, n_rep), shifted(t, dt, 2)
+        return remote(
+            column_parts.at[z, t], column_parts.at[at_z, at_t],
+            column_ssem.at[dz, dt], column_rsem.at[dz, dt],
+            (shifted(z, dz, n_rep), f, shifted(t, dt, 2)),
+        )
+
+    def row_power_copy(dz, df):
+        return remote(
+            row_parts.at[z, f], row_parts.at[z, f], row_ssem.at[dz, df], row_rsem.at[dz, df],
+            (shifted(z, dz, n_rep), shifted(f, df, n_fs), t),
+        )
+
+    def row_power_arrival(dz, df):
+        at_z, at_f = shifted(z, n_rep - dz, n_rep), shifted(f, n_fs - df, n_fs)
+        return remote(
+            row_parts.at[z, f], row_parts.at[at_z, at_f], row_ssem.at[dz, df],
+            row_rsem.at[dz, df], (shifted(z, dz, n_rep), shifted(f, df, n_fs), t),
+        )
+
+    column_peers = [(dz, dt) for dz in range(n_rep) for dt in range(2) if dz or dt]
+    row_peers = [(dz, df) for dz in range(n_rep) for df in range(n_fs) if dz or df]
+
+    own_sum(GATE)
+    relay(GATE, 1)
+    own_sum(UP)
+    for peer in column_peers:
+        column_copy(*peer).start()
+    for s in range(2, n_rep):
+        relay(GATE, s)
+    relay(UP, 1)
+    own_sum(DOWN)
+    for peer in row_peers:
+        row_power_copy(*peer).start()
+    for s in range(2, n_rep):
+        relay(UP, s)
+    for s in range(1, n_rep):
+        relay(DOWN, s)
+
+    grad_normed = normed_part[z, t]
+    for d in range(1, n_rep):
+        rep_copy(d).wait_recv()
+        grad_normed = grad_normed + rep_part[d]
+    normed_exact, recip_norm = normalise()
+    inner = jnp.sum(grad_normed * normed_exact, axis=1, keepdims=True) * (1.0 / width)
+    input_ref[...] = (recip_norm * (grad_normed - normed_exact * inner)).astype(jnp.bfloat16)
+
+    for peer in column_peers:
+        column_arrival(*peer).wait_recv()
+    for peer in row_peers:
+        row_power_arrival(*peer).wait_recv()
+    column_power[...] = jnp.sum(column_parts[...].reshape((2 * n_rep,) + column_parts.shape[2:]), axis=0)
+    row_power[...] = jnp.sum(row_parts[...], axis=1)
+
+    for which in (GATE, UP, DOWN):
+        for d in range(1, n_fs):
+            weight_copy(which, d).wait_send()
+            scatter_copy(which, d).wait_send()
+    for j in range(n_rep):
+        pair_copy(j, t).wait_send()
+        partner_copy(j).wait_send()
+
+        @pl.when((z < n_rep - 1) & (z >= j))
+        def _():
+            row_copy(j, rows_up, z).wait_send()
+            for which in (GATE, UP, DOWN):
+                gather_copy(which, j, gather_up, z).wait_send()
+
+        @pl.when((z > 0) & (z <= j))
+        def _():
+            row_copy(j, rows_down, z).wait_send()
+            for which in (GATE, UP, DOWN):
+                gather_copy(which, j, gather_down, z).wait_send()
+    for d in range(1, n_rep):
+        rep_copy(d).wait_send()
+    for peer in column_peers:
+        column_copy(*peer).wait_send()
+    for peer in row_peers:
+        row_power_copy(*peer).wait_send()
+
+
+def on_device_fused(n_rep, n_fs, tokens, cotangent, gate_weight, up_weight, down_weight):
+    local, width = tokens.shape
+    block, hidden_local = gate_weight.shape
+    units = hidden_local // n_rep
+    factor = 1.0 / math.sqrt(local * 2 * n_rep * n_fs)
+    start = lax.axis_index("rep") * units
+    gate_part = lax.dynamic_slice_in_dim(gate_weight, start, units, axis=1)
+    up_part = lax.dynamic_slice_in_dim(up_weight, start, units, axis=1)
+    down_part = lax.dynamic_slice_in_dim(down_weight, start, units, axis=0)
+    count = n_rep * 2 * local
+    f32, bf16 = jnp.float32, jnp.bfloat16
+    shapes = (
+        jax.ShapeDtypeStruct((local, width), bf16),
+        jax.ShapeDtypeStruct((n_rep, block, units), f32),
+        jax.ShapeDtypeStruct((n_rep, block, units), f32),
+        jax.ShapeDtypeStruct((n_rep, units, block), f32),
+        jax.ShapeDtypeStruct((2, 8, block), f32),
+        jax.ShapeDtypeStruct((n_rep, 8, units), f32),
+    )
+    dma = pltpu.SemaphoreType.DMA
+    vmem = pltpu.VMEM
+    scratch = [
+        vmem((n_rep, 2, 2, local, width), bf16),
+        vmem((n_fs, block, units), bf16),
+        vmem((n_fs, block, units), bf16),
+        vmem((n_fs, units, block), bf16),
+        vmem((count, units), bf16),
+        vmem((count, units), bf16),
+        vmem((count, units), bf16),
+        vmem((n_rep, 2, local, width), f32),
+        vmem((n_rep, local, width), f32),
+        vmem((n_rep, local, width), f32),
+        vmem((n_fs, block, units), f32),
+        vmem((n_fs, block, units), f32),
+        vmem((n_fs, units, block), f32),
+        vmem((n_fs, block, units), f32),
+        vmem((n_fs, block, units), f32),
+        vmem((n_fs, units, block), f32),
+        vmem((n_rep, 2, 2, 8, block), f32),
+        vmem((n_rep, n_fs, 8, units), f32),
+        dma((n_rep,)), dma((n_rep,)), dma((n_rep,)), dma((n_rep,)), dma((n_rep,)),
+        dma((3, n_fs)), dma((3, n_fs)),
+        dma((n_rep,)), dma((n_rep,)), dma((n_rep,)), dma((n_rep,)),
+        dma((3, n_fs)), dma((3, n_fs)),
+        dma((3, n_rep)), dma((3, n_rep)), dma((3, n_rep)),
+        dma((n_rep, 2)), dma((n_rep, 2)), dma((n_rep, n_fs)), dma((n_rep, n_fs)),
+    ]
+    whole = pl.BlockSpec(memory_space=pltpu.VMEM)
+    input_grad, gate_blocks, up_blocks, down_blocks, column_power, row_power = pl.pallas_call(
+        functools.partial(exchange_kernel, n_rep, n_fs, factor),
+        out_shape=shapes,
+        in_specs=[whole] * 5,
+        out_specs=(whole,) * 6,
+        scratch_shapes=scratch,
+        compiler_params=pltpu.CompilerParams(
+            collective_id=0, has_side_effects=True, vmem_limit_bytes=56 * 1024 * 1024
+        ),
+    )(tokens, cotangent, gate_part, up_part, down_part)
+    hidden_units = hidden_local * 2
+    return (
+        input_grad,
+        gate_blocks.transpose(1, 0, 2).reshape(block, hidden_local),
+        up_blocks.transpose(1, 0, 2).reshape(block, hidden_local),
+        down_blocks.reshape(hidden_local, block),
+        column_power[0, 0] / hidden_units,
+        column_power[1, 0] / hidden_units,
+        row_power[:, 0].reshape(hidden_local) / width,
+    )
+
+
 def solution(mesh):
     placed = (
         P(("rep", "fs", "tp"), None),
@@ -95,8 +523,12 @@
         P("fs", "tp"),
         P("tp", "fs"),
     )
+    n_rep, n_fs = mesh.shape["rep"], mesh.shape["fs"]
+    step = on_device
+    if mesh.shape["tp"] == 2 and FF // 2 % (16 * n_rep) == 0 and D % (128 * n_fs) == 0:
+        step = functools.partial(on_device_fused, n_rep, n_fs)
     return jax.shard_map(
-        on_device,
+        step,
         mesh=mesh,
         in_specs=placed,
         out_specs=(

time: 512 us -> 165 us (0.32)
  waiting for transfers between devices: 440 us -> 0 us
  Pallas kernels: 0 us -> 149 us
  blocking collectives: 16.6 us -> 0 us
  matrix products: 16 us -> 0 us
  other arithmetic: 17.8 us -> 2.11 us
  between operations: 14.2 us -> 0.68 us
  local copies, waits for them, and re-layouts: 5.81 us -> 13.4 us
    reduce_scatter x2 -> x0, waiting for transfers between devices: 163 us -> none  [the longest x1 152 us: on_device(): lax.psum_scatter(rows_term(), 'fs', scatter_dimension=0, tiled=True)]
    psum x1 -> x0, waiting for transfers between devices: 159 us -> none  [on_device(): reduced = lax.psum(reduced, 'rep')]
    pallas_call x0 -> x1, Pallas kernels: none -> 149 us  [on_device_fused(): pl.pallas_call(functools.partial(exchange_kernel, n_rep, n_fs, factor), o...]
    all_gather x3 -> x0, waiting for transfers between devices: 117 us -> none  [the longest x1 40.9 us: on_device(): lax.all_gather(up_weight, 'fs', axis=0, tiled=True)]
    dot_general x8 -> x0, matrix products: 16 us -> none  [the longest x3 5.35 us: contract_rows(): lax.dot_general(left, right, (((0,), (0,)), ((), ())), preferred_element_...]
    psum x2 -> x0, blocking collectives: 12.4 us -> none  [the longest x1 10 us: on_device(): down_sums = lax.psum(jnp.sum(down_grad * down_grad, axis=1), 'fs')]
    reduce_sum x4 -> x0, other arithmetic: 7.58 us -> none  [the longest x1 3.92 us: on_device(): jnp.sum(up_grad * up_grad, axis=1)]
    mul x1 -> x0, other arithmetic: 6.28 us -> none  [rows_term(): factor * jnp.concatenate([contract_rows(normed_cols, grad_gate_pre), cont...]
  transfers between devices with their start and end apart: 6 -> 0, of which waited for: 6 -> 0; matrix products, arithmetic and copies ran while one was open for 3% -> 0% of each run, Pallas kernels for 0% -> 0%
where the time goes in v1:
time: 165 us
  Pallas kernels  149 us (90%)
  local copies, waits for them, and re-layouts  13.4 us (8%)
  other arithmetic  2.11 us (1%)
    pallas_call x1, Pallas kernels, on_device_fused(): pl.pallas_call(functools.partial(exchange_kernel, n_rep, n_fs, factor), o...  149 us
    unnamed x8, local copies, waits for them, and re-layouts  6.3 us

profile of v1, /device:TPU:0, one launch (start us, length us, event | category | flops | bytes accessed | tf_op | source)
XLA Modules:
  0.0 165.1 jit_solution(12281388263807747812)
XLA Ops:
  0.6 0.0 copy-start
  0.7 2.0 %constant_dynamic-slice_fusion.1 = (bf16[256,352]{1,0:T(8,128)(2,1)}, bf16[256,352]{1,0:T(8,128)(2,1)}) fusion(bf16[256,1408]{1,0:T(8,128)(2,1)} %param.8, s32[]{:T(128)S(6)} %select_n.2, bf16[256,1408]{1,0:T(8,128)(2,1)} %param.7), kind=kLoop, calls=%fused_computation.4 | loop fusion | bytes 720900 | tf_op jit(solution)/shard_map/dynamic_slice | solution.py:455
  2.7 0.0 copy-done
  2.7 0.7 constant_dynamic-slice_fusion.down_ref
  3.4 148.8 %shard_map.108 = (bf16[64,1024]{1,0:T(8,128)(2,1)}, f32[4,256,352]{2,1,0:T(8,128)}, f32[4,256,352]{2,1,0:T(8,128)}, f32[4,352,256]{2,1,0:T(8,128)}, f32[2,8,256]{2,1,0:T(8,128)}, /*index=5*/f32[4,8,352]{2,1,0:T(8,128)}) custom-call(bf16[64,1024]{1,0:T(8,128)(2,1)} %tokens_ref.1, bf16[64,1024]{1,0:T(8,128)(2,1)} %cotangent_ref.1, ...), custom_call_target="tpu_custom_call" | custom-call | tf_op jit(solution)/shard_map/pallas_call | solution.py:496
  152.2 1.3 slice_multiply_fusion
  153.5 1.9 %copy.12 = f32[256,4,352]{0,2,1:T(8,128)S(1)} copy(f32[256,4,352]{2,0,1:T(8,128)} %bitcast.10) | data formatting | bytes 2883584 | tf_op jit(solution)/shard_map/transpose | solution.py:509
  155.4 1.5 copy.14
  156.9 1.9 %copy.13 = f32[256,4,352]{0,2,1:T(8,128)S(1)} copy(f32[256,4,352]{2,0,1:T(8,128)} %bitcast.9) | data formatting | bytes 2883584 | tf_op jit(solution)/shard_map/transpose | solution.py:510
  158.8 0.0 copy-start.1
  158.8 1.5 copy.15
  160.4 0.8 multiply_reduce_fusion
  161.2 0.7 div.24
  161.9 0.0 copy-done.1
  161.9 0.7 copy.18
  162.5 2.6 %copy.19 = f32[1408,256]{1,0:T(8,128)} copy(f32[1408,256]{1,0:T(8,128)} %bitcast.11) | data formatting | bytes 2883584
Async XLA Ops:
  0.6 2.1 %copy-start = (bf16[1408,256]{1,0:T(8,128)(2,1)S(1)}, bf16[1408,256]{1,0:T(8,128)(2,1)}, u32[]{:S(2)}) copy-start(bf16[1408,256]{1,0:T(8,128)(2,1)} %param.9) | copy-start | bytes 2162692
  158.8 3.1 %copy-start.1 = (bf16[64,1024]{1,0:T(8,128)(2,1)S(1)}, bf16[64,1024]{1,0:T(8,128)(2,1)}, u32[]{:S(2)}) copy-start(bf16[64,1024]{1,0:T(8,128)(2,1)} %get-tuple-element.37) | copy-start | bytes 393220

commit v2 on v1

--- a/solution.py
+++ b/solution.py
@@ -97,7 +97,7 @@
 def exchange_kernel(
     n_rep, n_fs, factor,
     tokens_ref, cotangent_ref, gate_ref, up_ref, down_ref,
-    input_ref, gate_out, up_out, down_out, column_power, row_power,
+    input_ref, gate_low, gate_high, up_low, up_high, down_low, down_high, column_power, row_power,
     rows_all, gate_all, up_all, down_all,
     grad_gate, grad_up, hidden_all,
     normed_part, partner_part, rep_part,
@@ -114,7 +114,7 @@
     other = 1 - t
     local, width = tokens_ref.shape
     block = gate_ref.shape[0]
-    hidden_units = gate_ref.shape[1]
+    hidden_units = gate_all.shape[2]
     chunk = 2 * local
 
     def remote(source, target, send_sem, recv_sem, where):
@@ -149,12 +149,17 @@
 
     rows_all[z, t, 0] = normalise()[0].astype(jnp.bfloat16)
     rows_all[z, t, 1] = cotangent_ref[...]
-    gate_all[f] = gate_ref[...]
-    up_all[f] = up_ref[...]
-    down_all[f] = down_ref[...]
+    for j in range(n_rep):
+        @pl.when(z == j)
+        def _():
+            gate_all[f] = gate_ref[:, j * hidden_units : (j + 1) * hidden_units]
+            up_all[f] = up_ref[:, j * hidden_units : (j + 1) * hidden_units]
+
+    units_at = pl.ds(pl.multiple_of(z * hidden_units, 16), hidden_units)
+    down_all[f] = down_ref[units_at, :]
     pl.semaphore_wait(barrier, n_rep * n_fs - 1 + n_rep)
 
-    weights = ((gate_ref, gate_all), (up_ref, up_all), (down_ref, down_all))
+    weights = ((gate_all.at[f], gate_all), (up_all.at[f], up_all), (down_ref.at[units_at], down_all))
 
     def weight_copy(which, d):
         source, target = weights[which]
@@ -302,13 +307,29 @@
     for which in (GATE, UP, DOWN):
         sums[which][0][0] = term(which, f)
 
-    outs = (gate_out, up_out, down_out)
-
-    def gather_copy(which, j, sems, to):
-        return remote(
-            outs[which].at[j], outs[which].at[j], sems.at[which, j], gather_rsem.at[which, j],
-            (to, f, t),
-        )
+    outs = ((gate_low, gate_high), (up_low, up_high), (down_low, down_high))
+
+    class gather_copy:
+        def __init__(self, which, j, sems, to):
+            self.pieces = [
+                remote(
+                    out.at[j], out.at[j], sems.at[which, part, j],
+                    gather_rsem.at[which, part, j], (to, f, t),
+                )
+                for part, out in enumerate(outs[which])
+            ]
+
+        def start(self):
+            for piece in self.pieces:
+                piece.start()
+
+        def wait_recv(self):
+            for piece in self.pieces:
+                piece.wait_recv()
+
+        def wait_send(self):
+            for piece in self.pieces:
+                piece.wait_send()
 
     def row_squares(value):
         return lax.dot_general(
@@ -324,7 +345,9 @@
             scatter_copy(which, d).wait_recv()
             total = total + target[d]
         total = total * (factor if which != DOWN else 0.5 * factor)
-        outs[which][z] = total
+        cut = outs[which][0].shape[1]
+        outs[which][0][z] = total[:cut].astype(jnp.bfloat16)
+        outs[which][1][z] = total[cut:]
 
         @pl.when(z < n_rep - 1)
         def _():
@@ -445,22 +468,41 @@
         row_power_copy(*peer).wait_send()
 
 
+def assemble_kernel(
+    n_rep, width,
+    gate_low, gate_high, up_low, up_high, down_low, down_high, column_power, row_power,
+    gate_out, up_out, down_out, gate_power, up_power, down_power,
+):
+    cut, units = gate_low.shape[1:]
+    down_cut = down_low.shape[1]
+    for j in range(n_rep):
+        at = slice(j * units, (j + 1) * units)
+        for low, high, out in ((gate_low, gate_high, gate_out), (up_low, up_high, up_out)):
+            out[:cut, at] = low[j].astype(jnp.float32)
+            out[cut:, at] = high[j]
+        down_out[j * units : j * units + down_cut, :] = down_low[j].astype(jnp.float32)
+        down_out[j * units + down_cut : (j + 1) * units, :] = down_high[j]
+        down_power[:, at] = row_power[j, 0:1] * (1.0 / width)
+    gate_power[...] = column_power[0, 0:1] * (1.0 / (2 * n_rep * units))
+    up_power[...] = column_power[1, 0:1] * (1.0 / (2 * n_rep * units))
+
+
 def on_device_fused(n_rep, n_fs, tokens, cotangent, gate_weight, up_weight, down_weight):
     local, width = tokens.shape
     block, hidden_local = gate_weight.shape
     units = hidden_local // n_rep
     factor = 1.0 / math.sqrt(local * 2 * n_rep * n_fs)
-    start = lax.axis_index("rep") * units
-    gate_part = lax.dynamic_slice_in_dim(gate_weight, start, units, axis=1)
-    up_part = lax.dynamic_slice_in_dim(up_weight, start, units, axis=1)
-    down_part = lax.dynamic_slice_in_dim(down_weight, start, units, axis=0)
     count = n_rep * 2 * local
+    cut, down_cut = block * 3 // 4 // 16 * 16, units * 3 // 4 // 16 * 16
     f32, bf16 = jnp.float32, jnp.bfloat16
     shapes = (
         jax.ShapeDtypeStruct((local, width), bf16),
-        jax.ShapeDtypeStruct((n_rep, block, units), f32),
-        jax.ShapeDtypeStruct((n_rep, block, units), f32),
-        jax.ShapeDtypeStruct((n_rep, units, block), f32),
+        jax.ShapeDtypeStruct((n_rep, cut, units), bf16),
+        jax.ShapeDtypeStruct((n_rep, block - cut, units), f32),
+        jax.ShapeDtypeStruct((n_rep, cut, units), bf16),
+        jax.ShapeDtypeStruct((n_rep, block - cut, units), f32),
+        jax.ShapeDtypeStruct((n_rep, down_cut, block), bf16),
+        jax.ShapeDtypeStruct((n_rep, units - down_cut, block), f32),
         jax.ShapeDtypeStruct((2, 8, block), f32),
         jax.ShapeDtypeStruct((n_rep, 8, units), f32),
     )
@@ -489,29 +531,37 @@
         dma((3, n_fs)), dma((3, n_fs)),
         dma((n_rep,)), dma((n_rep,)), dma((n_rep,)), dma((n_rep,)),
         dma((3, n_fs)), dma((3, n_fs)),
-        dma((3, n_rep)), dma((3, n_rep)), dma((3, n_rep)),
+        dma((3, 2, n_rep)), dma((3, 2, n_rep)), dma((3, 2, n_rep)),
         dma((n_rep, 2)), dma((n_rep, 2)), dma((n_rep, n_fs)), dma((n_rep, n_fs)),
     ]
     whole = pl.BlockSpec(memory_space=pltpu.VMEM)
-    input_grad, gate_blocks, up_blocks, down_blocks, column_power, row_power = pl.pallas_call(
+    input_grad, *blocks = pl.pallas_call(
         functools.partial(exchange_kernel, n_rep, n_fs, factor),
         out_shape=shapes,
         in_specs=[whole] * 5,
-        out_specs=(whole,) * 6,
+        out_specs=(whole,) * 9,
         scratch_shapes=scratch,
         compiler_params=pltpu.CompilerParams(
             collective_id=0, has_side_effects=True, vmem_limit_bytes=56 * 1024 * 1024
         ),
-    )(tokens, cotangent, gate_part, up_part, down_part)
-    hidden_units = hidden_local * 2
+    )(tokens, cotangent, gate_weight, up_weight, down_weight)
+    gate_grad, up_grad, down_grad, gate_power, up_power, down_power = pl.pallas_call(
+        functools.partial(assemble_kernel, n_rep, width),
+        out_shape=(
+            jax.ShapeDtypeStruct((block, hidden_local), f32),
+            jax.ShapeDtypeStruct((block, hidden_local), f32),
+            jax.ShapeDtypeStruct((hidden_local, block), f32),
+            jax.ShapeDtypeStruct((1, block), f32),
+            jax.ShapeDtypeStruct((1, block), f32),
+            jax.ShapeDtypeStruct((1, hidden_local), f32),
+        ),
+        in_specs=[whole] * 8,
+        out_specs=(whole,) * 6,
+        compiler_params=pltpu.CompilerParams(vmem_limit_bytes=32 * 1024 * 1024),
+    )(*blocks)
     return (
-        input_grad,
-        gate_blocks.transpose(1, 0, 2).reshape(block, hidden_local),
-        up_blocks.transpose(1, 0, 2).reshape(block, hidden_local),
-        down_blocks.reshape(hidden_local, block),
-        column_power[0, 0] / hidden_units,
-        column_power[1, 0] / hidden_units,
-        row_power[:, 0].reshape(hidden_local) / width,
+        input_grad, gate_grad, up_grad, down_grad,
+        gate_power.reshape(block), up_power.reshape(block), down_power.reshape(hidden_local),
     )
 
 

time: 165 us -> 137 us (0.83)
  Pallas kernels: 149 us -> 126 us
  local copies, waits for them, and re-layouts: 13.4 us -> 8.32 us
    pallas_call x1, Pallas kernels: 149 us -> 124 us  [on_device_fused(): pl.pallas_call(functools.partial(exchange_kernel, n_rep, n_fs, factor), o...]
    transpose x2 -> x0, local copies, waits for them, and re-layouts: 3.73 us -> none  [the longest x1 1.86 us: on_device_fused(): gate_blocks.transpose(1, 0, 2).reshape(block, hidden_local)]
    dynamic_slice x2 -> x0, local copies, waits for them, and re-layouts: 2.73 us -> none  [the longest x1 2.05 us: on_device_fused(): up_part = lax.dynamic_slice_in_dim(up_weight, start, units, axis=1)]
    pallas_call x0 -> x1, Pallas kernels: none -> 2.47 us  [on_device_fused(): pl.pallas_call(functools.partial(assemble_kernel, n_rep, width), out_shap...]
    div x2 -> x0, other arithmetic: 2.11 us -> none  [the longest x1 1.28 us: on_device_fused(): column_power[1, 0] / hidden_units]
    unnamed x8 -> x19, local copies, waits for them, and re-layouts: 6.3 us -> 8.32 us
where the time goes in v2:
time: 137 us; the launch traced here: 136 us
  Pallas kernels  126 us (92%)
  local copies, waits for them, and re-layouts  8.32 us (6%)
    pallas_call x1, Pallas kernels, on_device_fused(): pl.pallas_call(functools.partial(exchange_kernel, n_rep, n_fs, factor), o...  124 us
    unnamed x19, local copies, waits for them, and re-layouts  8.32 us

profile of v2, /device:TPU:0, one launch (start us, length us, event | category | flops | bytes accessed | tf_op | source)
XLA Modules:
  0.0 136.1 jit_solution(17636986667396361721)
XLA Ops:
  0.6 124.0 %shard_map.108 = (bf16[64,1024]{1,0:T(8,128)(2,1)}, bf16[4,192,352]{2,1,0:T(8,128)(2,1)}, f32[4,64,352]{2,1,0:T(8,128)}, bf16[4,192,352]{2,1,0:T(8,128)(2,1)}, f...) custom-call(bf16[64,1024]{1,0:T(8,128)(2,1)} %tokens_ref.1, ...), custom_call_target="tpu_custom_call" | custom-call | tf_op jit(solution)/shard_map/pallas_call | solution.py:538
  124.7 0.0 copy-start
  124.7 1.1 copy-done
  125.7 0.0 copy-start.1
  125.7 1.1 copy-done.1
  126.8 0.0 copy-start.2
  126.8 1.0 copy-done.2
  127.8 0.0 copy-start.3
  127.8 1.0 copy-done.3
  128.8 0.0 copy-start.4
  128.8 1.0 copy-done.4
  129.8 0.0 copy-start.5
  129.8 1.0 copy-done.5
  130.8 0.0 copy-start.6
  130.8 0.8 copy-done.6
  131.6 0.0 copy-start.7
  131.6 0.7 copy-done.7
  132.3 0.0 copy-start.8
  132.3 2.5 %shard_map.109 = (f32[256,1408]{1,0:T(8,128)}, f32[256,1408]{1,0:T(8,128)}, f32[1408,256]{1,0:T(8,128)}, f32[1,256]{1,0:T(1,128)}, f32[1,256]{1,0:T(1,128)}, /*index=5*/f32[1,1408]{1,0:T(1,128)S(1)}) custom-call(bf16[4,192,352]{2,1,0:T(8,128)(2,1)S(1)} %copy-done, f32[4,64,352]{2,1,0:T(8,128)S(1)} %copy-done.3, bf16[4,192,352]{2,1,0:T(8,128)(2,1)S(1)} %copy-done.1, ...), custom_call_target="tpu_custom_call" | custom-call | tf_op jit(solution)/shard_map/pallas_call | solution.py:548
  134.8 0.6 reduce
  135.4 0.0 copy-done.8
  135.4 0.7 copy.13
Async XLA Ops:
  124.7 1.1 copy-start
  125.7 1.1 copy-start.1
  126.8 1.0 copy-start.2
  127.8 1.0 copy-start.3
  128.8 1.0 copy-start.4
  129.8 1.0 copy-start.5
  130.8 0.8 copy-start.6
  131.6 0.7 copy-start.7
  132.3 3.1 %copy-start.8 = (bf16[64,1024]{1,0:T(8,128)(2,1)S(1)}, bf16[64,1024]{1,0:T(8,128)(2,1)}, u32[]{:S(2)}) copy-start(bf16[64,1024]{1,0:T(8,128)(2,1)} %get-tuple-element.44) | copy-start | bytes 393220

commit v3 on v2

--- a/solution.py
+++ b/solution.py
@@ -112,6 +112,10 @@
 ):
     z, f, t = lax.axis_index("rep"), lax.axis_index("fs"), lax.axis_index("tp")
     other = 1 - t
+    side_x = f + 1 - 2 * lax.rem(f, 2)
+    side_y = lax.rem(f + 2, n_fs)
+    across = lax.rem(side_x + 2, n_fs)
+    sides = (side_x, side_y)
     local, width = tokens_ref.shape
     block = gate_ref.shape[0]
     hidden_units = gate_all.shape[2]
@@ -161,19 +165,43 @@
 
     weights = ((gate_all.at[f], gate_all), (up_all.at[f], up_all), (down_ref.at[units_at], down_all))
 
-    def weight_copy(which, d):
+    def weight_copy(which, side):
         source, target = weights[which]
         return remote(
-            source, target.at[f], weight_ssem.at[which, d], weight_rsem.at[which, d],
-            (z, shifted(f, d, n_fs), t),
-        )
-
-    def weight_arrival(which, d):
-        source, target = weights[which]
-        return remote(
-            source, target.at[shifted(f, n_fs - d, n_fs)],
-            weight_ssem.at[which, d], weight_rsem.at[which, d], (z, shifted(f, d, n_fs), t),
-        )
+            source, target.at[f], weight_ssem.at[which, side], weight_rsem.at[which, side],
+            (z, sides[side], t),
+        )
+
+    def weight_arrival(which, side):
+        target = weights[which][1].at[sides[side]]
+        return remote(
+            target, target, weight_ssem.at[which, side], weight_rsem.at[which, side],
+            (z, sides[side], t),
+        )
+
+    def half_of(which, part):
+        rows = weights[which][1].shape[1] // 2
+        return pl.ds(part * rows, rows)
+
+    def weight_forward(which, side):
+        origin = sides[1 - side]
+        part = weights[which][1].at[origin, half_of(which, 1 - side)]
+        return remote(
+            part, part, weight_ssem.at[which, 2 + side], weight_rsem.at[which, 2 + side],
+            (z, sides[side], t),
+        )
+
+    def weight_across(which, side):
+        part = weights[which][1].at[across, half_of(which, 1 - side)]
+        return remote(
+            part, part, weight_ssem.at[which, 2 + side], weight_rsem.at[which, 2 + side],
+            (z, sides[side], t),
+        )
+
+    def pass_weights(which):
+        for side in (0, 1):
+            weight_arrival(which, side).wait_recv()
+            weight_forward(which, 1 - side).start()
 
     def row_copy(j, sems, to):
         return remote(
@@ -195,11 +223,16 @@
         row_copy(z, rows_down, z - 1).start()
 
     for which in (GATE, UP, DOWN):
-        for d in range(1, n_fs):
-            weight_copy(which, d).start()
+        for side in (0, 1):
+            weight_copy(which, side).start()
     pair_copy(z, t).start()
 
-    for s in range(1, n_rep):
+    for s in range(1, max(n_rep, 4)):
+        if s <= 3:
+            pass_weights(s - 1)
+        if s >= n_rep:
+            continue
+
         @pl.when(z - s >= 0)
         def _():
             row_copy(z - s, rows_up, z).wait_recv()
@@ -221,8 +254,8 @@
     for j in range(n_rep):
         pair_copy(j, other).wait_recv()
     for which in (GATE, UP, DOWN):
-        for d in range(1, n_fs):
-            weight_arrival(which, d).wait_recv()
+        for side in (0, 1):
+            weight_across(which, side).wait_recv()
 
     def forward(j, carry):
         normed = rows_all[j, :, 0].reshape(chunk, width)
@@ -247,23 +280,24 @@
         ).astype(jnp.bfloat16)
         grad_up[at, :] = grad_up_pre
         grad_gate[at, :] = grad_gate_pre
+        return carry
+
+    lax.fori_loop(0, n_rep, forward, 0)
+
+    def backward(j, carry):
+        at = pl.ds(pl.multiple_of(j * chunk, chunk), chunk)
         for k in range(n_fs):
-            part = contract_cols(grad_gate_pre, gate_all[k]) + contract_cols(
-                grad_up_pre, up_all[k]
+            part = contract_cols(grad_gate[at, :], gate_all[k]) + contract_cols(
+                grad_up[at, :], up_all[k]
             )
             normed_part[j, :, :, k * block : (k + 1) * block] = part.reshape(2, local, block)
         return carry
 
-    lax.fori_loop(0, n_rep, forward, 0)
-
     def partner_copy(j):
         return remote(
             normed_part.at[j, other], partner_part.at[j], partner_ssem.at[j], partner_rsem.at[j],
             (z, f, other),
         )
-
-    for j in range(n_rep):
-        partner_copy(j).start()
 
     def columns_of(half, k):
         at = pl.ds(pl.multiple_of(k * block, block), block)
@@ -278,17 +312,44 @@
 
     sums = ((gate_send, gate_recv), (up_send, up_recv), (down_send, down_recv))
 
-    def scatter_copy(which, d):
+    def half(which, part):
+        rows = sums[which][0].shape[1] // 2
+        return pl.ds(part * rows, rows)
+
+    def scatter_copy(which, side, kind):
         source, target = sums[which]
-        return remote(
-            source.at[d], target.at[d], scatter_ssem.at[which, d], scatter_rsem.at[which, d],
-            (z, shifted(f, d, n_fs), t),
+        at = half(which, side)
+        slot = (1 + side) if kind == 0 else 3
+        sem = 2 * side + kind
+        return remote(
+            source.at[slot, at], target.at[kind, at],
+            scatter_ssem.at[which, sem], scatter_rsem.at[which, sem], (z, sides[side], t),
+        )
+
+    def pass_copy(which, side):
+        source, target = sums[which]
+        at = half(which, 1 - side)
+        return remote(
+            source.at[1 + side, at], target.at[2, at],
+            scatter_ssem.at[which, 4 + side], scatter_rsem.at[which, 4 + side],
+            (z, sides[side], t),
         )
 
     def send_terms(which):
-        for d in range(1, n_fs):
-            sums[which][0][d] = term(which, shifted(f, d, n_fs))
-            scatter_copy(which, d).start()
+        sums[which][0][3] = term(which, across)
+        for side in (0, 1):
+            scatter_copy(which, side, 1).start()
+        for side in (0, 1):
+            sums[which][0][1 + side] = term(which, sides[side])
+            scatter_copy(which, side, 0).start()
+
+    def pass_sums(which):
+        source, target = sums[which]
+        for side in (0, 1):
+            scatter_copy(which, 1 - side, 1).wait_recv()
+            at = half(which, 1 - side)
+            source[1 + side, at] = source[1 + side, at] + target[1, at]
+            pass_copy(which, side).start()
 
     def rep_copy(d):
         return remote(
@@ -297,14 +358,19 @@
         )
 
     send_terms(GATE)
+    lax.fori_loop(0, n_rep, backward, 0)
+    for j in range(n_rep):
+        partner_copy(j).start()
+    send_terms(UP)
     for j in range(n_rep):
         partner_copy(j).wait_recv()
         normed_part[j, t] = normed_part[j, t] + partner_part[j]
     for d in range(1, n_rep):
         rep_copy(d).start()
-    send_terms(UP)
+    sums[GATE][0][0] = term(GATE, f)
+    pass_sums(GATE)
     send_terms(DOWN)
-    for which in (GATE, UP, DOWN):
+    for which in (UP, DOWN):
         sums[which][0][0] = term(which, f)
 
     outs = ((gate_low, gate_high), (up_low, up_high), (down_low, down_high))
@@ -340,10 +406,10 @@
 
     def own_sum(which):
         source, target = sums[which]
-        total = source[0]
-        for d in range(1, n_fs):
-            scatter_copy(which, d).wait_recv()
-            total = total + target[d]
+        for side in (0, 1):
+            scatter_copy(which, side, 0).wait_recv()
+            pass_copy(which, side).wait_recv()
+        total = source[0] + target[0] + target[2]
         total = total * (factor if which != DOWN else 0.5 * factor)
         cut = outs[which][0].shape[1]
         outs[which][0][z] = total[:cut].astype(jnp.bfloat16)
@@ -411,7 +477,9 @@
     row_peers = [(dz, df) for dz in range(n_rep) for df in range(n_fs) if dz or df]
 
     own_sum(GATE)
+    pass_sums(UP)
     relay(GATE, 1)
+    pass_sums(DOWN)
     own_sum(UP)
     for peer in column_peers:
         column_copy(*peer).start()
@@ -442,9 +510,12 @@
     row_power[...] = jnp.sum(row_parts[...], axis=1)
 
     for which in (GATE, UP, DOWN):
-        for d in range(1, n_fs):
-            weight_copy(which, d).wait_send()
-            scatter_copy(which, d).wait_send()
+        for side in (0, 1):
+            weight_copy(which, side).wait_send()
+            weight_forward(which, side).wait_send()
+            scatter_copy(which, side, 0).wait_send()
+            scatter_copy(which, side, 1).wait_send()
+            pass_copy(which, side).wait_send()
     for j in range(n_rep):
         pair_copy(j, t).wait_send()
         partner_copy(j).wait_send()
@@ -528,9 +599,9 @@
         vmem((n_rep, 2, 2, 8, block), f32),
         vmem((n_rep, n_fs, 8, units), f32),
         dma((n_rep,)), dma((n_rep,)), dma((n_rep,)), dma((n_rep,)), dma((n_rep,)),
-        dma((3, n_fs)), dma((3, n_fs)),
+        dma((3, 4)), dma((3, 4)),
         dma((n_rep,)), dma((n_rep,)), dma((n_rep,)), dma((n_rep,)),
-        dma((3, n_fs)), dma((3, n_fs)),
+        dma((3, 6)), dma((3, 6)),
         dma((3, 2, n_rep)), dma((3, 2, n_rep)), dma((3, 2, n_rep)),
         dma((n_rep, 2)), dma((n_rep, 2)), dma((n_rep, n_fs)), dma((n_rep, n_fs)),
     ]
@@ -542,7 +613,7 @@
         out_specs=(whole,) * 9,
         scratch_shapes=scratch,
         compiler_params=pltpu.CompilerParams(
-            collective_id=0, has_side_effects=True, vmem_limit_bytes=56 * 1024 * 1024
+            collective_id=0, has_side_effects=True, vmem_limit_bytes=63 * 1024 * 1024
         ),
     )(tokens, cotangent, gate_weight, up_weight, down_weight)
     gate_grad, up_grad, down_grad, gate_power, up_power, down_power = pl.pallas_call(
@@ -557,7 +628,7 @@
         ),
         in_specs=[whole] * 8,
         out_specs=(whole,) * 6,
-        compiler_params=pltpu.CompilerParams(vmem_limit_bytes=32 * 1024 * 1024),
+        compiler_params=pltpu.CompilerParams(vmem_limit_bytes=63 * 1024 * 1024),
     )(*blocks)
     return (
         input_grad, gate_grad, up_grad, down_grad,
@@ -575,7 +646,7 @@
     )
     n_rep, n_fs = mesh.shape["rep"], mesh.shape["fs"]
     step = on_device
-    if mesh.shape["tp"] == 2 and FF // 2 % (16 * n_rep) == 0 and D % (128 * n_fs) == 0:
+    if mesh.shape["tp"] == 2 and n_fs == 4 and FF // 2 % (16 * n_rep) == 0 and D % (128 * n_fs) == 0:
         step = functools.partial(on_device_fused, n_rep, n_fs)
     return jax.shard_map(
         step,

time: 137 us -> 124 us (0.905)
  local copies, waits for them, and re-layouts: 8.32 us -> 0.66 us
  Pallas kernels: 126 us -> 121 us
    unnamed x19 -> x3, local copies, waits for them, and re-layouts: 8.32 us -> 0.66 us
    pallas_call x1, Pallas kernels: 124 us -> 116 us  [on_device_fused(): pl.pallas_call(functools.partial(exchange_kernel, n_rep, n_fs, factor), o...]
    pallas_call x1, Pallas kernels: 2.47 us -> 4.27 us  [on_device_fused(): pl.pallas_call(functools.partial(assemble_kernel, n_rep, width), out_shap...]
where the time goes in v3:
time: 124 us; the launch traced here: 123 us
  Pallas kernels  121 us (98%)
  other arithmetic  1.31 us (1%)
    pallas_call x1, Pallas kernels, on_device_fused(): pl.pallas_call(functools.partial(exchange_kernel, n_rep, n_fs, factor), o...  116 us
    pallas_call x1, Pallas kernels, on_device_fused(): pl.pallas_call(functools.partial(assemble_kernel, n_rep, width), out_shap...  4.27 us

profile of v3, /device:TPU:0, one launch (start us, length us, event | category | flops | bytes accessed | tf_op | source)
XLA Modules:
  0.0 123.4 jit_solution(13793855051997552207)
XLA Ops:
  0.6 116.5 %shard_map.108 = (bf16[64,1024]{1,0:T(8,128)(2,1)}, bf16[4,192,352]{2,1,0:T(8,128)(2,1)}, f32[4,64,352]{2,1,0:T(8,128)}, bf16[4,192,352]{2,1,0:T(8,128)(2,1)}, f...) custom-call(bf16[64,1024]{1,0:T(8,128)(2,1)} %tokens_ref.1, ...), custom_call_target="tpu_custom_call" | custom-call | tf_op jit(solution)/shard_map/pallas_call | solution.py:609
  117.1 0.0 copy-start
  117.1 4.3 %shard_map.109 = (f32[256,1408]{1,0:T(8,128)}, f32[256,1408]{1,0:T(8,128)}, f32[1408,256]{1,0:T(8,128)}, f32[1,256]{1,0:T(1,128)}, f32[1,256]{1,0:T(1,128)}, /*index=5*/f32[1,1408]{1,0:T(1,128)}) custom-call(bf16[4,192,352]{2,1,0:T(8,128)(2,1)} %get-tuple-element.23.gate_low, f32[4,64,352]{2,1,0:T(8,128)} %get-tuple-element.24.gate_high, ...), custom_call_target="tpu_custom_call" | custom-call | tf_op jit(solution)/shard_map/pallas_call | solution.py:619
  121.4 1.3 %reduce = f32[1408]{0:T(1024)} reduce(f32[1,1408]{1,0:T(1,128)} %get-tuple-element.36, f32[]{:T(128)} %constant), dimensions={0}, to_apply=%get-tuple-element.36.reduce_sub_computation | reduce | bytes 11268 | tf_op jit(solution)/shard_map/pallas_call | solution.py:619
  122.7 0.0 copy-done
  122.7 0.7 copy.13
Async XLA Ops:
  117.1 5.6 %copy-start = (bf16[64,1024]{1,0:T(8,128)(2,1)S(1)}, bf16[64,1024]{1,0:T(8,128)(2,1)}, u32[]{:S(2)}) copy-start(bf16[64,1024]{1,0:T(8,128)(2,1)} %get-tuple-element.44) | copy-start | bytes 393220

commit v4 on v3

--- a/solution.py
+++ b/solution.py
@@ -429,21 +429,24 @@
             column_parts[z, t, which] = row_squares(total)
 
     def relay(which, s):
-        @pl.when(z - s >= 0)
+        @pl.when((z - s >= 0) & (z < n_rep - 1))
         def _():
             gather_copy(which, z - s, gather_up, z).wait_recv()
-
-            @pl.when(z < n_rep - 1)
-            def _():
-                gather_copy(which, z - s, gather_up, z + 1).start()
-
-        @pl.when(z + s < n_rep)
+            gather_copy(which, z - s, gather_up, z + 1).start()
+
+        @pl.when((z + s < n_rep) & (z > 0))
         def _():
             gather_copy(which, z + s, gather_down, z).wait_recv()
-
-            @pl.when(z > 0)
-            def _():
-                gather_copy(which, z + s, gather_down, z - 1).start()
+            gather_copy(which, z + s, gather_down, z - 1).start()
+
+    def collect(which, s):
+        @pl.when((z - s >= 0) & (z == n_rep - 1))
+        def _():
+            gather_copy(which, z - s, gather_up, z).wait_recv()
+
+        @pl.when((z + s < n_rep) & (z == 0))
+        def _():
+            gather_copy(which, z + s, gather_down, z).wait_recv()
 
     def column_copy(dz, dt):
         return remote(
@@ -483,15 +486,14 @@
     own_sum(UP)
     for peer in column_peers:
         column_copy(*peer).start()
-    for s in range(2, n_rep):
+    for s in range(2, n_rep - 1):
         relay(GATE, s)
-    relay(UP, 1)
     own_sum(DOWN)
     for peer in row_peers:
         row_power_copy(*peer).start()
-    for s in range(2, n_rep):
+    for s in range(1, n_rep - 1):
         relay(UP, s)
-    for s in range(1, n_rep):
+    for s in range(1, n_rep - 1):
         relay(DOWN, s)
 
     grad_normed = normed_part[z, t]
@@ -502,6 +504,9 @@
     inner = jnp.sum(grad_normed * normed_exact, axis=1, keepdims=True) * (1.0 / width)
     input_ref[...] = (recip_norm * (grad_normed - normed_exact * inner)).astype(jnp.bfloat16)
 
+    for which in (GATE, UP, DOWN):
+        for s in range(1, n_rep):
+            collect(which, s)
     for peer in column_peers:
         column_arrival(*peer).wait_recv()
     for peer in row_peers:
@@ -645,9 +650,15 @@
         P("tp", "fs"),
     )
     n_rep, n_fs = mesh.shape["rep"], mesh.shape["fs"]
-    step = on_device
-    if mesh.shape["tp"] == 2 and n_fs == 4 and FF // 2 % (16 * n_rep) == 0 and D % (128 * n_fs) == 0:
-        step = functools.partial(on_device_fused, n_rep, n_fs)
+
+    def step(tokens, cotangent, gate_weight, up_weight, down_weight):
+        block, hidden_local = gate_weight.shape
+        run = on_device
+        if mesh.shape["tp"] == 2 and n_fs == 4:
+            if hidden_local % (16 * n_rep) == 0 and block % 128 == 0:
+                run = functools.partial(on_device_fused, n_rep, n_fs)
+        return run(tokens, cotangent, gate_weight, up_weight, down_weight)
+
     return jax.shard_map(
         step,
         mesh=mesh,

time: 124 us -> 123 us (level)
  no operation moved by 1% of the time
where the time goes in v4:
time: 123 us
  Pallas kernels  121 us (98%)
  other arithmetic  1.31 us (1%)
    pallas_call x1, Pallas kernels, on_device_fused(): pl.pallas_call(functools.partial(exchange_kernel, n_rep, n_fs, factor), o...  116 us
    pallas_call x1, Pallas kernels, on_device_fused(): pl.pallas_call(functools.partial(assemble_kernel, n_rep, width), out_shap...  4.27 us

profile of v4, /device:TPU:0, one launch (start us, length us, event | category | flops | bytes accessed | tf_op | source)
XLA Modules:
  0.0 123.1 jit_solution(7016617361262021884)
XLA Ops:
  0.6 116.3 %shard_map.108 = (bf16[64,1024]{1,0:T(8,128)(2,1)}, bf16[4,192,352]{2,1,0:T(8,128)(2,1)}, f32[4,64,352]{2,1,0:T(8,128)}, bf16[4,192,352]{2,1,0:T(8,128)(2,1)}, f...) custom-call(bf16[64,1024]{1,0:T(8,128)(2,1)} %tokens_ref.1, ...), custom_call_target="tpu_custom_call" | custom-call | tf_op jit(solution)/shard_map/pallas_call | solution.py:614
  116.9 0.0 copy-start
  116.9 4.3 %shard_map.109 = (f32[256,1408]{1,0:T(8,128)}, f32[256,1408]{1,0:T(8,128)}, f32[1408,256]{1,0:T(8,128)}, f32[1,256]{1,0:T(1,128)}, f32[1,256]{1,0:T(1,128)}, /*index=5*/f32[1,1408]{1,0:T(1,128)}) custom-call(bf16[4,192,352]{2,1,0:T(8,128)(2,1)} %get-tuple-element.23.gate_low, f32[4,64,352]{2,1,0:T(8,128)} %get-tuple-element.24.gate_high, ...), custom_call_target="tpu_custom_call" | custom-call | tf_op jit(solution)/shard_map/pallas_call | solution.py:624
  121.2 1.3 %reduce = f32[1408]{0:T(1024)} reduce(f32[1,1408]{1,0:T(1,128)} %get-tuple-element.36, f32[]{:T(128)} %constant), dimensions={0}, to_apply=%get-tuple-element.36.reduce_sub_computation | reduce | bytes 11268 | tf_op jit(solution)/shard_map/pallas_call | solution.py:624
  122.5 0.0 copy-done
  122.5 0.7 copy.13
Async XLA Ops:
  116.9 5.6 %copy-start = (bf16[64,1024]{1,0:T(8,128)(2,1)S(1)}, bf16[64,1024]{1,0:T(8,128)(2,1)}, u32[]{:S(2)}) copy-start(bf16[64,1024]{1,0:T(8,128)(2,1)} %get-tuple-element.44) | copy-start | bytes 393220

commit v5 on v4

--- a/solution.py
+++ b/solution.py
@@ -305,9 +305,9 @@
 
     def term(which, k):
         if which == GATE:
-            return contract_rows(columns_of(0, k), grad_gate[...])
+            return contract_rows(grad_gate[...], columns_of(0, k))
         if which == UP:
-            return contract_rows(columns_of(0, k), grad_up[...])
+            return contract_rows(grad_up[...], columns_of(0, k))
         return contract_rows(hidden_all[...], columns_of(1, k))
 
     sums = ((gate_send, gate_recv), (up_send, up_recv), (down_send, down_recv))
@@ -426,7 +426,8 @@
         if which == DOWN:
             row_parts[z, f] = row_squares(total)
         else:
-            column_parts[z, t, which] = row_squares(total)
+            squares = jnp.sum(total * total, axis=0, keepdims=True)
+            column_parts[z, t, which] = jnp.broadcast_to(squares, (8, block))
 
     def relay(which, s):
         @pl.when((z - s >= 0) & (z < n_rep - 1))
@@ -549,15 +550,15 @@
     gate_low, gate_high, up_low, up_high, down_low, down_high, column_power, row_power,
     gate_out, up_out, down_out, gate_power, up_power, down_power,
 ):
-    cut, units = gate_low.shape[1:]
-    down_cut = down_low.shape[1]
+    cut = gate_low.shape[1]
+    units = cut + gate_high.shape[1]
     for j in range(n_rep):
         at = slice(j * units, (j + 1) * units)
         for low, high, out in ((gate_low, gate_high, gate_out), (up_low, up_high, up_out)):
-            out[:cut, at] = low[j].astype(jnp.float32)
-            out[cut:, at] = high[j]
-        down_out[j * units : j * units + down_cut, :] = down_low[j].astype(jnp.float32)
-        down_out[j * units + down_cut : (j + 1) * units, :] = down_high[j]
+            both = jnp.concatenate([low[j].astype(jnp.float32), high[j]], axis=0)
+            out[:, at] = both.T
+        down_out[j * units : j * units + cut, :] = down_low[j].astype(jnp.float32)
+        down_out[j * units + cut : (j + 1) * units, :] = down_high[j]
         down_power[:, at] = row_power[j, 0:1] * (1.0 / width)
     gate_power[...] = column_power[0, 0:1] * (1.0 / (2 * n_rep * units))
     up_power[...] = column_power[1, 0:1] * (1.0 / (2 * n_rep * units))
@@ -569,16 +570,14 @@
     units = hidden_local // n_rep
     factor = 1.0 / math.sqrt(local * 2 * n_rep * n_fs)
     count = n_rep * 2 * local
-    cut, down_cut = block * 3 // 4 // 16 * 16, units * 3 // 4 // 16 * 16
+    cut = units * 13 // 16 // 16 * 16
     f32, bf16 = jnp.float32, jnp.bfloat16
     shapes = (
         jax.ShapeDtypeStruct((local, width), bf16),
-        jax.ShapeDtypeStruct((n_rep, cut, units), bf16),
-        jax.ShapeDtypeStruct((n_rep, block - cut, units), f32),
-        jax.ShapeDtypeStruct((n_rep, cut, units), bf16),
-        jax.ShapeDtypeStruct((n_rep, block - cut, units), f32),
-        jax.ShapeDtypeStruct((n_rep, down_cut, block), bf16),
-        jax.ShapeDtypeStruct((n_rep, units - down_cut, block), f32),
+        *[
+            jax.ShapeDtypeStruct((n_rep, cut, block), bf16),
+            jax.ShapeDtypeStruct((n_rep, units - cut, block), f32),
+        ] * 3,
         jax.ShapeDtypeStruct((2, 8, block), f32),
         jax.ShapeDtypeStruct((n_rep, 8, units), f32),
     )
@@ -595,12 +594,7 @@
         vmem((n_rep, 2, local, width), f32),
         vmem((n_rep, local, width), f32),
         vmem((n_rep, local, width), f32),
-        vmem((n_fs, block, units), f32),
-        vmem((n_fs, block, units), f32),
-        vmem((n_fs, units, block), f32),
-        vmem((n_fs, block, units), f32),
-        vmem((n_fs, block, units), f32),
-        vmem((n_fs, units, block), f32),
+        *[vmem((n_fs, units, block), f32)] * 6,
         vmem((n_rep, 2, 2, 8, block), f32),
         vmem((n_rep, n_fs, 8, units), f32),
         dma((n_rep,)), dma((n_rep,)), dma((n_rep,)), dma((n_rep,)), dma((n_rep,)),

time: 123 us -> 120 us (0.976)
  Pallas kernels: 121 us -> 117 us
    pallas_call x1, Pallas kernels: 116 us -> 113 us  [on_device_fused(): pl.pallas_call(functools.partial(exchange_kernel, n_rep, n_fs, factor), o...]
where the time goes in v5:
time: 120 us
  Pallas kernels  117 us (98%)
  other arithmetic  1.31 us (1%)
    pallas_call x1, Pallas kernels, on_device_fused(): pl.pallas_call(functools.partial(exchange_kernel, n_rep, n_fs, factor), o...  113 us
    pallas_call x1, Pallas kernels, on_device_fused(): pl.pallas_call(functools.partial(assemble_kernel, n_rep, width), out_shap...  4.75 us

profile of v5, /device:TPU:0, one launch (start us, length us, event | category | flops | bytes accessed | tf_op | source)
XLA Modules:
  0.0 120.1 jit_solution(4642710209871313960)
XLA Ops:
  0.6 112.7 %shard_map.108 = (bf16[64,1024]{1,0:T(8,128)(2,1)}, bf16[4,272,256]{2,1,0:T(8,128)(2,1)}, f32[4,80,256]{2,1,0:T(8,128)}, bf16[4,272,256]{2,1,0:T(8,128)(2,1)}, f...) custom-call(bf16[64,1024]{1,0:T(8,128)(2,1)} %tokens_ref.1, ...), custom_call_target="tpu_custom_call" | custom-call | tf_op jit(solution)/shard_map/pallas_call | solution.py:608
  113.3 0.0 copy-start
  113.4 4.8 %shard_map.109 = (f32[256,1408]{1,0:T(8,128)}, f32[256,1408]{1,0:T(8,128)}, f32[1408,256]{1,0:T(8,128)}, f32[1,256]{1,0:T(1,128)}, f32[1,256]{1,0:T(1,128)}, /*index=5*/f32[1,1408]{1,0:T(1,128)}) custom-call(bf16[4,272,256]{2,1,0:T(8,128)(2,1)} %get-tuple-element.23.gate_low, f32[4,80,256]{2,1,0:T(8,128)} %get-tuple-element.24.gate_high, ...), custom_call_target="tpu_custom_call" | custom-call | tf_op jit(solution)/shard_map/pallas_call | solution.py:618
  118.1 1.3 %reduce = f32[1408]{0:T(1024)} reduce(f32[1,1408]{1,0:T(1,128)} %get-tuple-element.36, f32[]{:T(128)} %constant), dimensions={0}, to_apply=%get-tuple-element.36.reduce_sub_computation | reduce | bytes 11268 | tf_op jit(solution)/shard_map/pallas_call | solution.py:618
  119.4 0.0 copy-done
  119.4 0.7 copy.13
Async XLA Ops:
  113.3 6.1 %copy-start = (bf16[64,1024]{1,0:T(8,128)(2,1)S(1)}, bf16[64,1024]{1,0:T(8,128)(2,1)}, u32[]{:S(2)}) copy-start(bf16[64,1024]{1,0:T(8,128)(2,1)} %get-tuple-element.44) | copy-start | bytes 393220
